TPU v7x, 32 devices: a whole 2x2x4 slice. The times are simulated.
32 devices in a mesh: sp: 4 (over y, x), tp: 8 (over z, core).
Axes of the slice: x: 2, y: 2, z: 4, core: 2. Of those that a mesh axis runs over, the one named last changes fastest.
Arguments:
- query_input: bfloat16 [1024, 1024], P('tp', 'sp'), may hold values from -6 to 6
- key_input: bfloat16 [1024, 1024], P('tp', 'sp'), may hold values from -6 to 6
- retrieved_content_matrix: bfloat16 [1024, 1024], P('tp', 'sp'), may hold values from -6 to 6
- gate_input: bfloat16 [1024, 1024], P('tp', 'sp'), may hold values from -6 to 6
- log_decay: float32 [2, 16, 1024], P(None, 'tp', 'sp'), may hold values from -2 to 0
- residual: bfloat16 [1024, 2048], P(('sp', 'tp')), may hold values from -6 to 6
- out_weight: bfloat16 [1024, 2048], replicated, may hold values from -0.1875 to 0.1875
- norm_gain: bfloat16 [2048], replicated, may hold values from 0.099609375 to 1.8984375
- routes: int32 [1024, 2], P(('sp', 'tp')), may hold values from 0 to 3, all different within a row; in each aligned block of 32 rows (0 to 31, 32 to 63, ...) at most 20 rows name the same one
- route_weight: float32 [1024, 2], P(('sp', 'tp')), may hold values from 0.1 to 1
- gate_weight: bfloat16 [4, 2048, 5504], P('sp', None, 'tp'), may hold values from -0.125 to 0.125
- up_weight: bfloat16 [4, 2048, 5504], P('sp', None, 'tp'), may hold values from -0.125 to 0.125
- down_weight: bfloat16 [4, 5504, 2048], P('sp', 'tp'), may hold values from -0.078125 to 0.078125
Outputs:
- output: bfloat16 [1024, 2048], P(('sp', 'tp'))
Inputs may be any that keep to these rules, and one draw needn't show every extreme that they name: `routes`: each row names 2 different experts. In each aligned block of 32 rows no expert is named by more than 20 rows, a bound that some block reaches.
All inputs are finite; a program needn't handle non-finite values.
Results may differ from a plain program's by a relative error of at most 0.015.
Values may be sent and summed in bfloat16 or wider, within the bound.
A program may use at most 64 MiB of HBM per device.

v0:
```python
import jax
import jax.numpy as jnp
from jax import lax
from jax.sharding import PartitionSpec as P

HEAD_DIM = 64


full_precision = lax.Precision.HIGHEST


def entering(value, axis, join, neutral, backward):
    count, mine = (lax.axis_size(axis), lax.axis_index(axis))
    pieces = jax.tree.map(lambda part: lax.all_gather(part, axis), value)
    if backward:
        pieces = jax.tree.map(lambda part: part[::-1], pieces)
        mine = count - 1 - mine
    total = jax.tree.map(
        lambda part, zero: jnp.full_like(part, 0) + jnp.asarray(zero, part.dtype), value, neutral
    )

    def turn(position, total):
        longer = join(total, jax.tree.map(lambda part: part[position], pieces))
        return jax.tree.map(lambda new, old: jnp.where(position < mine, new, old), longer, total)

    return lax.fori_loop(0, count - 1, turn, total)


def head_norm(values, mesh_axis):
    centred = values - jnp.mean(values, axis=mesh_axis, keepdims=True)
    return centred * lax.rsqrt(jnp.mean(centred * centred, axis=mesh_axis, keepdims=True) + 1e-06)


def join_states(earlier, later):
    return (earlier[0] + later[0], later[1] + jnp.exp(later[0])[..., None, None] * earlier[1])


def on_device(
    query_input,
    key_input,
    retrieved_content_matrix,
    gate_input,
    log_decay,
    residual,
    out_weight,
    norm_gain,
    routes,
    route_weight,
    gate_weight,
    up_weight,
    down_weight,
):
    heads_here = query_input.shape[0] // HEAD_DIM
    length = query_input.shape[1]
    queries = query_input.reshape(heads_here, HEAD_DIM, length)
    all_keys = key_input.reshape(heads_here, HEAD_DIM, length)
    all_values = retrieved_content_matrix.reshape(heads_here, HEAD_DIM, length)
    forward_log = log_decay[0]
    backward_log = log_decay[1]
    forward_prefix = jnp.cumsum(forward_log, axis=-1)
    backward_prefix = jnp.cumsum(backward_log, axis=-1) - backward_log
    forward_total = forward_prefix[:, -1]
    backward_total = jnp.sum(backward_log, axis=-1)
    wide_keys = all_keys.astype(jnp.float32)
    wide_values = all_values.astype(jnp.float32)
    forward_keys = wide_keys * jnp.exp(forward_total[:, None] - forward_prefix)[:, None, :]
    backward_keys = wide_keys * jnp.exp(backward_prefix)[:, None, :]
    local_forward = jnp.einsum("hds,hes->hde", forward_keys, wide_values, precision=full_precision)
    backward_local = jnp.einsum(
        "hds,hes->hde", backward_keys, wide_values, precision=full_precision
    )
    identity = (jnp.zeros_like(forward_total), jnp.zeros_like(local_forward))
    _, forward_in = entering((forward_total, local_forward), "sp", join_states, identity, False)
    _, backward_in = entering((backward_total, backward_local), "sp", join_states, identity, True)
    block_size = min(512, length)
    block_count = length // block_size
    offsets = jnp.arange(length)

    def block_output(block):
        start = block * block_size
        places_here = start + jnp.arange(block_size)
        scores = jnp.einsum("hdt,hds->hts", queries, all_keys, preferred_element_type=jnp.float32)
        before = places_here[:, None] >= offsets[None, :]
        after = places_here[:, None] <= offsets[None, :]
        forward_decay_weight = jnp.exp(
            jnp.where(before, forward_prefix[:, :, None] - forward_prefix[:, None, :], -jnp.inf)
        )
        backward_weight = jnp.exp(
            jnp.where(after, backward_prefix[:, None, :] - backward_prefix[:, :, None], -jnp.inf)
        )
        weighted = (scores * (forward_decay_weight + backward_weight)).astype(jnp.bfloat16)
        inner = jnp.einsum("hts,hes->het", weighted, all_values, preferred_element_type=jnp.float32)
        query_wide = queries.astype(jnp.float32)
        carried = (
            jnp.einsum("hdt,hde->het", query_wide, forward_in, precision=full_precision)
            * jnp.exp(forward_prefix)[:, None, :]
        )
        carried = (
            carried
            + jnp.einsum("hdt,hde->het", query_wide, backward_in, precision=full_precision)
            * jnp.exp(backward_total[:, None] - backward_prefix)[:, None, :]
        )
        return inner + carried

    blocks = lax.map(block_output, jnp.arange(block_count))
    retained = jnp.transpose(blocks, (1, 2, 0, 3)).reshape(heads_here, HEAD_DIM, length)
    gate_values = gate_input.reshape(heads_here, HEAD_DIM, length).astype(jnp.float32)
    mixer_out = (
        (head_norm(retained, 1) * jax.nn.silu(gate_values))
        .reshape(heads_here * HEAD_DIM, length)
        .astype(jnp.bfloat16)
    )
    token_major = lax.all_to_all(mixer_out, "tp", split_axis=1, concat_axis=0, tiled=True)
    projected = lax.dot_general(
        token_major, out_weight, (((0,), (0,)), ((), ())), preferred_element_type=jnp.float32
    )
    stream = residual.astype(jnp.float32) + projected
    scale = lax.rsqrt(jnp.mean(stream * stream, axis=-1, keepdims=True) + 1e-06)
    normed = (stream * scale * norm_gain.astype(jnp.float32)).astype(jnp.bfloat16)
    token_count = routes.shape[0]
    picks = routes.shape[1]
    width = normed.shape[1]
    experts_all = lax.axis_size("sp") * gate_weight.shape[0]
    capacity = (5 * token_count + 2 * experts_all - 1) // (2 * experts_all)
    flat_routes = routes.reshape(-1)
    matches = (flat_routes[:, None] == jnp.arange(experts_all)[None, :]).astype(jnp.int32)
    ranks = jnp.cumsum(matches, axis=0) - matches
    bucket_ordinal = jnp.sum(ranks * matches, axis=1)
    target = flat_routes * capacity + bucket_ordinal
    slot_grid = jnp.arange(experts_all * capacity)
    placing = (slot_grid[:, None] == target[None, :]).astype(jnp.int32)
    placing = jnp.sum(placing.reshape(experts_all * capacity, token_count, picks), axis=2).astype(
        jnp.bfloat16
    )
    send_rows = jnp.dot(placing, normed, preferred_element_type=jnp.float32).astype(jnp.bfloat16)
    send_rows = send_rows.reshape(experts_all, capacity, width)
    received = lax.all_to_all(send_rows, "sp", split_axis=0, concat_axis=0, tiled=True)
    piece = lax.all_gather(received, "tp", axis=0, tiled=True)
    flat_rows = piece.reshape(-1, piece.shape[-1])
    gates = jnp.dot(flat_rows, gate_weight[0], preferred_element_type=jnp.float32)
    ups = jnp.dot(flat_rows, up_weight[0], preferred_element_type=jnp.float32)
    hidden = (jax.nn.silu(gates) * ups).astype(jnp.bfloat16)
    partial_out = jnp.dot(hidden, down_weight[0], preferred_element_type=jnp.float32).astype(
        jnp.bfloat16
    )
    partial_out = lax.optimization_barrier(partial_out)
    terms = partial_out.astype(jnp.float32).reshape(piece.shape)
    summed = lax.psum_scatter(terms.astype(jnp.bfloat16), "tp", scatter_dimension=0, tiled=True)
    returned = lax.all_to_all(summed, "sp", split_axis=0, concat_axis=0, tiled=True)
    flat_back = returned.reshape(experts_all * capacity, width)
    picked_rows = jnp.take(flat_back, target, axis=0).reshape(token_count, picks, width)
    combined = jnp.sum(route_weight[:, :, None] * picked_rows.astype(jnp.float32), axis=1)
    return (stream + combined).astype(jnp.bfloat16)


def solution(mesh):
    placed = (
        P("tp", "sp"),
        P("tp", "sp"),
        P("tp", "sp"),
        P("tp", "sp"),
        P(None, "tp", "sp"),
        P(("sp", "tp"), None),
        P(),
        P(),
        P(("sp", "tp"), None),
        P(("sp", "tp"), None),
        P("sp", None, "tp"),
        P("sp", None, "tp"),
        P("sp", "tp", None),
    )
    return jax.shard_map(
        on_device, mesh=mesh, in_specs=placed, out_specs=P(("sp", "tp"), None), check_vma=False
    )
```

profile of v0, /device:TPU:25, one launch (start us, length us, event | category | flops | bytes accessed | tf_op | source)
XLA Modules:
  0.0 202.2 jit_solution(16112550918665750718)
XLA Ops:
  6.5 0.7 iota_compare_fusion
  7.2 1.0 fusion.51
  8.2 0.6 reduce-window.14
  8.8 0.2 slice_reduce_fusion.1
  9.0 0.2 reduce-window.15
  9.3 0.1 copy.57
  9.4 1.3 dynamic-slice
  11.3 0.1 bitcast_dynamic-update-slice_fusion
  11.4 0.2 dynamic-update-slice.1
  11.6 8.4 %all-reduce.2 = (f32[8]{0:T(128)S(1)}, f32[8]{0:T(128)}) all-reduce(f32[8]{0:T(128)S(1)} %dynamic-update-slice.1, f32[8]{0:T(128)S(1)} %bitcast_dynamic-update-slice_fusion), channel_id=5, replica_groups=mesh['sp'=4,'tp'=8] {'sp'}, use_global_device_ids=true, to_apply=%add.1 | all-reduce | flops 16 | bytes 128
  20.0 0.1 reshape.288
  20.2 0.6 reduce-window.16
  20.8 0.2 slice_reduce_fusion
  20.9 0.2 reduce-window.19
  21.2 0.8 subtract_exponential_fusion
  22.0 0.6 copy-done.6
  22.5 1.1 fusion.31
  23.6 6.0 %all-gather.2 = f32[8,64,64]{2,1,0:T(8,128)S(1)} all-gather(f32[2,64,64]{2,1,0:T(8,128)S(1)} %fusion.31), channel_id=4, replica_groups=mesh['sp'=4,'tp'=8] {'sp'}, dimensions={0}, use_global_device_ids=true | all-gather | bytes 163840 | tf_op jit(solution)/shard_map/all_gather | solution.py:14
  29.7 0.3 while.33
  29.7 0.1 fusion.69
  29.8 0.1 fusion.69
  29.9 0.1 fusion.69
  30.0 0.8 fusion.49
  30.8 1.1 fusion.30
  31.9 7.2 %all-gather = f32[8,64,64]{2,1,0:T(8,128)S(1)} all-gather(f32[2,64,64]{2,1,0:T(8,128)S(1)} %fusion.30), channel_id=2, replica_groups=mesh['sp'=4,'tp'=8] {'sp'}, dimensions={0}, use_global_device_ids=true | all-gather | bytes 163840 | tf_op jit(solution)/shard_map/all_gather | solution.py:14
  39.1 0.7 reshape.286
  39.8 0.3 while.32
  39.8 0.1 fusion.68
  40.1 0.3 convolution_multiply_fusion.1
  40.4 0.3 fusion.13
  40.7 1.4 fusion.52
  42.1 0.9 fusion.38
  43.0 0.1 copy.48
  43.1 0.7 convert_element_type.68
  43.9 11.1 %all-to-all-start = ((bf16[128,8,32]{0,2,1:T(8,128)(2,1)}), bf16[128,8,32]{0,2,1:T(8,128)(2,1)S(1)}, u32[]{:S(2)}, u32[]{:S(2)}) async-start(bf16[128,8,32]{0,2,1:T(8,128)(2,1)} %convert_element_type.68), calls=%async_computation | async-start | bytes 131072 | tf_op jit(solution)/shard_map/all_to_all | solution.py:113
  55.0 0.1 copy.51
  55.1 0.1 reshape.272
  55.3 0.1 reduce_window_sum.68
  55.4 0.2 select_reduce_fusion
  55.6 0.1 reduce_sum.71
  55.9 1.7 all-to-all-done
  57.6 3.1 %multiply_reduce_fusion.1 = (f32[32]{0:T(128)S(1)}, f32[32,2048]{1,0:T(8,128)S(1)}) fusion(bf16[1024,2048]{1,0:T(8,128)(2,1)} %param.23, bf16[32,2048]{1,0:T(8,128)(2,1)} %param.22, bf16[128,8,32]{0,2,1:T(8,128)(2,1)S(1)} %all-to-all-done), kind=kOutput, calls=%fused_computation.35 | convolution fusion | flops 134479840 | bytes 4653184 | tf_op jit(solution)/shard_map/dot_general | solution.py:114
  60.8 0.3 convolution_convert_fusion.1
  61.1 0.8 reshape.273
  61.9 10.0 %all_to_all.26 = bf16[4,20,2048]{2,1,0:T(8,128)(2,1)} all-to-all(bf16[4,20,2048]{2,1,0:T(8,128)(2,1)} %reshape.273), channel_id=1, replica_groups=mesh['sp'=4,'tp'=8] {'sp'}, dimensions={0} | all-to-all | bytes 655360 | tf_op jit(solution)/shard_map/all_to_all | solution.py:137
  71.9 0.2 reduce-scatter.2.cloned.1.call-start
  72.2 37.5 %all-gather.6.cloned.1.call-done = bf16[32,20,2048]{2,1,0:T(8,128)(2,1)} async-done(((bf16[4,20,2048]{2,1,0:T(8,128)(2,1)}), bf16[32,20,2048]{2,1,0:T(8,128)(2,1)}) %all-gather.6.cloned.1.call-update) | async-done | bytes 2621456 | tf_op jit(solution)/shard_map/all_gather | solution.py:138
  109.7 5.2 %reshape.274 = bf16[640,2048]{1,0:T(8,128)(2,1)} reshape(bf16[32,20,2048]{2,1,0:T(8,128)(2,1)} %all-gather.6.cloned.1.call-done) | data formatting | bytes 5242880 | tf_op jit(solution)/shard_map/reshape | solution.py:139
  114.8 6.2 %fusion.5 = f32[640,688]{0,1:T(8,128)} fusion(bf16[640,2048]{1,0:T(8,128)(2,1)} %reshape.274, bf16[1,2048,688]{1,2,0:T(8,128)(2,1)} %param.27), kind=kOutput, calls=%fused_computation.11 | convolution fusion | flops 1803550720 | bytes 7200768 | tf_op jit(solution)/shard_map/dot_general | solution.py:140
  121.0 13.0 %convolution_convert_fusion = bf16[640,2048]{1,0:T(8,128)(2,1)} fusion(bf16[1,688,2048]{2,1,0:T(8,128)(2,1)S(1)} %copy-done, f32[640,688]{0,1:T(8,128)} %fusion.5, bf16[640,2048]{1,0:T(8,128)(2,1)} %reshape.274, bf16[1,2048,688]{1,2,0:T(8,128)(2,1)} %param.28), kind=kOutput, calls=%fused_computation.7 | convolution fusion | flops 3611054080 | bytes 12640256 | tf_op jit(solution)/shard_map/dot_general | solution.py:143
  134.0 5.2 %convert_element_type.77 = bf16[32,20,2048]{2,1,0:T(8,128)(2,1)} reshape(bf16[640,2048]{1,0:T(8,128)(2,1)} %convolution_convert_fusion) | data formatting | bytes 5242880 | tf_op jit(solution)/shard_map/convert_element_type | solution.py:148
  139.2 0.1 copy.54
  139.3 0.1 mul.193
  139.4 0.1 copy.53
  139.5 0.3 copy-done.9
  139.9 0.1 copy.50
  140.0 39.2 %reduce-scatter.2.cloned.1.call-done = bf16[4,20,2048]{2,1,0:T(8,128)(2,1)} async-done(((bf16[32,20,2048]{2,1,0:T(8,128)(2,1)}), bf16[4,20,2048]{2,1,0:T(8,128)(2,1)}) %reduce-scatter.2.cloned.1.call-update) | async-done | bytes 327696 | tf_op jit(solution)/shard_map/reduce_scatter | solution.py:148
  179.2 4.1 %all-to-all-start.2 = ((bf16[4,20,2048]{2,1,0:T(8,128)(2,1)}), bf16[4,20,2048]{2,1,0:T(8,128)(2,1)}, u32[]{:S(2)}, u32[]{:S(2)}) async-start(bf16[4,20,2048]{2,1,0:T(8,128)(2,1)} %reduce-scatter.2.cloned.1.call-done), calls=%async_computation.3 | async-start | bytes 786432 | tf_op jit(solution)/shard_map/all_to_all | solution.py:149
  183.3 6.0 %all-to-all-done.2 = bf16[4,20,2048]{2,1,0:T(8,128)(2,1)} async-done(((bf16[4,20,2048]{2,1,0:T(8,128)(2,1)}), bf16[4,20,2048]{2,1,0:T(8,128)(2,1)}, u32[]{:S(2)}, u32[]{:S(2)}) %all-to-all-start.2) | async-done | bytes 327712 | tf_op jit(solution)/shard_map/all_to_all | solution.py:149
  189.3 1.1 reshape.275
  190.4 1.4 gather_fusion
  191.9 1.1 gather.7
  193.0 1.7 multiply_reduce_fusion
  194.7 0.7 add_convert_fusion
  (56 shorter events, 0.9 us)
Async XLA Ops:
  6.5 114.5 %copy-start = (bf16[1,688,2048]{2,1,0:T(8,128)(2,1)S(1)}, bf16[1,688,2048]{2,1,0:T(8,128)(2,1)}, u32[]{:S(2)}) copy-start(bf16[1,688,2048]{2,1,0:T(8,128)(2,1)} %param.29) | copy-start | bytes 8454148
  6.5 34.1 %copy-start.1 = (bf16[128,256]{1,0:T(8,128)(2,1)S(1)}, bf16[128,256]{1,0:T(8,128)(2,1)}, u32[]{:S(2)}) copy-start(bf16[128,256]{1,0:T(8,128)(2,1)} %param.19) | copy-start | bytes 196612
  9.2 10.8 %copy-start.7 = (f32[1,2,2,128]{3,1,2,0:T(2,128)}, f32[1,2,2,128]{3,1,2,0:T(2,128)S(1)}, u32[]{:S(2)}) copy-start(f32[1,2,2,128]{3,1,2,0:T(2,128)S(1)} %copy.74) | copy-start | bytes 6148
  9.4 12.5 %copy-start.10 = (f32[2,1]{0,1:T(1,128)}, f32[2,1]{0,1:T(1,128)S(1)}, u32[]{:S(2)}) copy-start(f32[2,1]{0,1:T(1,128)S(1)} %copy.57) | copy-start | bytes 28
  21.9 0.6 copy-start.6
  29.6 10.5 %copy-start.3 = (bf16[128,256]{1,0:T(8,128)(2,1)S(1)}, bf16[128,256]{1,0:T(8,128)(2,1)}, u32[]{:S(2)}) copy-start(bf16[128,256]{1,0:T(8,128)(2,1)} %param.17) | copy-start | bytes 196612
  29.6 11.0 %copy-start.2 = (bf16[128,256]{1,0:T(8,128)(2,1)S(1)}, bf16[128,256]{1,0:T(8,128)(2,1)}, u32[]{:S(2)}) copy-start(bf16[128,256]{1,0:T(8,128)(2,1)} %param.18) | copy-start | bytes 196612
  29.7 11.0 %copy-start.4 = (pred[256,256]{1,0:T(8,128)(4,1)S(1)}, pred[256,256]{1,0:T(8,128)(4,1)}, u32[]{:S(2)}) copy-start(pred[256,256]{1,0:T(8,128)(4,1)} %get-tuple-element.299) | copy-start | bytes 196612
  30.0 25.0 %copy-start.5 = (s32[32,2]{0,1:T(2,128)S(1)}, s32[32,2]{0,1:T(2,128)}, u32[]{:S(2)}) copy-start(s32[32,2]{0,1:T(2,128)} %param.25) | copy-start | bytes 772
  31.8 24.0 %copy-start.8 = (bf16[2048]{0:T(1024)(128)(2,1)S(1)}, bf16[2048]{0:T(1024)(128)(2,1)}, u32[]{:S(2)}) copy-start(bf16[2048]{0:T(1024)(128)(2,1)} %param.24) | copy-start | bytes 12292
  43.9 13.7 %all-to-all-start = ((bf16[128,8,32]{0,2,1:T(8,128)(2,1)}), bf16[128,8,32]{0,2,1:T(8,128)(2,1)S(1)}, u32[]{:S(2)}, u32[]{:S(2)}) async-start(bf16[128,8,32]{0,2,1:T(8,128)(2,1)} %convert_element_type.68), calls=%async_computation | async-start | bytes 131072 | tf_op jit(solution)/shard_map/all_to_all | solution.py:113
  55.0 54.6 %all-gather.6.cloned.1.call-start = ((), (), s32[]{:S(2)}) async-start(), calls=%async_computation.4 | async-start | bytes 3538944 | tf_op jit(solution)/shard_map/all_gather | solution.py:138
  71.9 107.2 %reduce-scatter.2.cloned.1.call-start = ((), (), s32[]{:S(2)}) async-start(), calls=%async_computation.5 | async-start | bytes 3538944 | tf_op jit(solution)/shard_map/reduce_scatter | solution.py:148
  139.2 0.7 copy-start.9
  179.2 10.2 %all-to-all-start.2 = ((bf16[4,20,2048]{2,1,0:T(8,128)(2,1)}), bf16[4,20,2048]{2,1,0:T(8,128)(2,1)}, u32[]{:S(2)}, u32[]{:S(2)}) async-start(bf16[4,20,2048]{2,1,0:T(8,128)(2,1)} %reduce-scatter.2.cloned.1.call-done), calls=%async_computation.3 | async-start | bytes 786432 | tf_op jit(solution)/shard_map/all_to_all | solution.py:149
Sparse Core Ops, SparseCore 0:
  72.1 37.5 all-gather.5
  139.3 39.7 reduce-scatter.1
where the time goes:
time: 206 us; the launch traced here: 202 us
  waiting for transfers between devices  84.5 us (41%)
  blocking collectives  31.7 us (15%)
  matrix products  26.6 us (13%)
  local copies, waits for them, and re-layouts  20.4 us (10%)
  starting transfers between devices  15.5 us (8%)
  between operations  14.3 us (7%)
  other arithmetic  9.16 us (4%)
    reduce_scatter x1, waiting for transfers between devices, on_device(): lax.psum_scatter(terms.astype(jnp.bfloat16), 'tp', scatter_dimension=0, t...  39.2 us
    all_gather x1, waiting for transfers between devices, on_device(): piece = lax.all_gather(received, 'tp', axis=0, tiled=True)  37.5 us
    all_gather x2, blocking collectives, entering(): pieces = jax.tree.map(lambda part: lax.all_gather(part, axis), value)  13.2 us
    dot_general x1, matrix products, on_device(): jnp.dot(hidden, down_weight[0], preferred_element_type=jnp.float32)  13 us
    all_to_all x1, starting transfers between devices, on_device(): lax.all_to_all(mixer_out, 'tp', split_axis=1, concat_axis=0, tiled=True)  11.1 us
    all_to_all x1, blocking collectives, on_device(): lax.all_to_all(send_rows, 'sp', split_axis=0, concat_axis=0, tiled=True)  10 us
    unnamed x1, blocking collectives  8.44 us
    dot_general x1, matrix products, on_device(): jnp.dot(flat_rows, gate_weight[0], preferred_element_type=jnp.float32)  6.18 us
  transfers between devices with their start and end apart: 4, of which 4 were waited for; matrix products, arithmetic and copies ran while one was open for 1% of the time, Pallas kernels for 0%

commit v1 on v0

v1 whole, which is shorter than its diff:
```python
import functools

import jax
import jax.numpy as jnp
from jax import lax
from jax.experimental import pallas as pl
from jax.experimental.pallas import tpu as pltpu
from jax.sharding import PartitionSpec as P

HEAD_DIM = 64
HIGH = lax.Precision.HIGHEST
F32 = jnp.float32
BF16 = jnp.bfloat16
NN = (((1,), (0,)), ((), ()))
NT = (((1,), (1,)), ((), ()))
TN = (((0,), (0,)), ((), ()))


def dot(a, b, dims=NN, precision=None):
    return lax.dot_general(a, b, dims, precision=precision, preferred_element_type=F32)


def kernel(
    n_sp, n_tp, slots,
    q_ref, k_ref, v_ref, g_ref, ld_ref, rt_ref, res_ref, ng_ref, wo_hbm, wg_hbm, wu_hbm, wd_hbm,
    out_ref,
    wo, wg, wu, wd, st, yg, res, rts, stream, normed, sel, xs, xr, pw, pr, rs, rr, zacc, zs, zr,
    wsem, st_s, st_r, y_s, y_r, res_s, res_r, rt_s, rt_r, x_s, x_r, f_s, f_r, p_s, p_r, b_s, b_r, z_s, z_r,
):
    sp, tp = lax.axis_index("sp"), lax.axis_index("tp")
    chips = n_tp // 2
    chip, core = tp // 2, lax.rem(tp, 2)
    partner = chip * 2 + 1 - core
    feats, length = q_ref.shape
    heads = feats // HEAD_DIM
    tok = res_ref.shape[0]
    half = wo.shape[1] // 2

    def remote(src, dst, send, recv, to_sp, to_tp):
        return pltpu.make_async_remote_copy(
            src_ref=src, dst_ref=dst, send_sem=send, recv_sem=recv,
            device_id=(to_sp, to_tp), device_id_type=pl.DeviceIdType.MESH,
        )

    loads = []
    for i, (a, b) in enumerate(((wo_hbm, wo), (wg_hbm.at[0], wg), (wu_hbm.at[0], wu), (wd_hbm.at[0], wd))):
        loads.append(pltpu.make_async_copy(a, b, wsem.at[i]))
        loads[-1].start()

    barrier = pltpu.get_barrier_semaphore()
    for d in range(1, n_tp):
        pl.semaphore_signal(barrier, inc=1, device_id=(sp, lax.rem(tp + d, n_tp)), device_id_type=pl.DeviceIdType.MESH)
    for d in range(1, n_sp):
        pl.semaphore_signal(barrier, inc=1, device_id=(lax.rem(sp + d, n_sp), tp), device_id_type=pl.DeviceIdType.MESH)

    def slot_tp(d, c):
        return lax.rem(chip + d + chips, chips) * 2 + c

    def gather_start(at, own, send, recv):
        for d in range(1, chips):
            remote(own, at(tp), send.at[d - 1], recv.at[tp], sp, slot_tp(d, core)).start()
        remote(own, at(tp), send.at[chips - 1], recv.at[tp], sp, partner).start()

    def gather_forward(at, own, send, recv):
        for d in range(1, chips):
            source = slot_tp(-d, core)
            remote(own, at(source), send.at[d - 1], recv.at[source], sp, partner).wait_recv()
            remote(at(source), at(source), send.at[chips - 1 + d], recv.at[source], sp, partner).start()

    def gather_finish(at, own, send, recv):
        for d in range(chips):
            source = slot_tp(-d, 1 - core)
            remote(own, at(source), send.at[d], recv.at[source], sp, partner).wait_recv()

    def gather_drain(at, own, send, recv):
        for d in range(2 * chips - 1):
            remote(own, at(tp), send.at[d], recv.at[tp], sp, partner).wait_send()

    def res_at(i):
        return res.at[pl.ds(pl.multiple_of(i * tok, tok), tok)]

    def y_at(i):
        return yg.at[pl.ds(pl.multiple_of(i * feats, feats), feats)]

    pl.semaphore_wait(barrier, n_tp - 1 + n_sp - 1)
    res_args = (res_at, res_ref, res_s, res_r)
    gather_start(*res_args)
    rt_copies = []
    for d in range(1, n_tp):
        to = lax.rem(tp + d, n_tp)
        c = remote(rt_ref, rts.at[tp], rt_s.at[d - 1], rt_r.at[tp], sp, to)
        c.start()
        rt_copies.append(c)
    rts[tp] = rt_ref[...]
    res[pl.ds(pl.multiple_of(tp * tok, tok), tok)] = res_ref[...]

    row = lax.broadcasted_iota(jnp.int32, (length, length), 0)
    col = lax.broadcasted_iota(jnp.int32, (length, length), 1)
    ld = ld_ref[...]
    upto = dot(ld, (row <= col).astype(F32), precision=HIGH)
    before = upto - ld
    upto_t, before_t = upto.T, before.T
    lane = lax.broadcasted_iota(jnp.int32, (8, 2 * HEAD_DIM), 1)
    for h in range(heads):
        cf, eb = upto[h:h + 1], before[heads + h:heads + h + 1]
        a_sum, b_sum = upto[h:h + 1, length - 1:], upto[heads + h:heads + h + 1, length - 1:]
        keys = k_ref[h * HEAD_DIM:(h + 1) * HEAD_DIM].astype(F32)
        values = v_ref[h * HEAD_DIM:(h + 1) * HEAD_DIM].astype(F32)
        both = jnp.concatenate([keys * jnp.exp(a_sum - cf), keys * jnp.exp(eb)], axis=0)
        st[sp, h, 0:HEAD_DIM] = dot(values, both, NT, HIGH)
        st[sp, h, HEAD_DIM:HEAD_DIM + 8] = jnp.where(lane < HEAD_DIM, a_sum, b_sum)
    st_copies = []
    for d in range(1, n_sp):
        to = lax.rem(sp + d, n_sp)
        c = remote(st.at[sp], st.at[sp], st_s.at[d - 1], st_r.at[sp], to, tp)
        c.start()
        st_copies.append(c)

    inner = []
    for h in range(heads):
        rows = slice(h * HEAD_DIM, (h + 1) * HEAD_DIM)
        scores = dot(q_ref[rows], k_ref[rows], TN)
        cf, cf_t = upto[h:h + 1], upto_t[:, h:h + 1]
        eb, eb_t = before[heads + h:heads + h + 1], before_t[:, heads + h:heads + h + 1]
        weight = jnp.exp(jnp.where(row >= col, cf_t - cf, -jnp.inf))
        weight = weight + jnp.exp(jnp.where(row <= col, eb - eb_t, -jnp.inf))
        inner.append(dot(v_ref[rows], (scores * weight).astype(BF16), NT))

    gather_forward(*res_args)
    for d in range(1, n_sp):
        source = lax.rem(sp + d, n_sp)
        remote(st.at[source], st.at[source], st_s.at[d - 1], st_r.at[source], source, tp).wait_recv()
    wide = lax.broadcasted_iota(jnp.int32, (1, 2 * HEAD_DIM), 1) < HEAD_DIM
    for h in range(heads):
        rows = slice(h * HEAD_DIM, (h + 1) * HEAD_DIM)
        cf, eb = upto[h:h + 1], before[heads + h:heads + h + 1]
        b_sum = upto[heads + h:heads + h + 1, length - 1:]
        totals = [st[m, h, HEAD_DIM:HEAD_DIM + 1] for m in range(n_sp)]
        state = jnp.zeros((HEAD_DIM, 2 * HEAD_DIM), F32)
        for m in range(n_sp):
            gap = jnp.zeros((1, 2 * HEAD_DIM), F32)
            for j in range(n_sp):
                if j > m:
                    gap = gap + jnp.where(wide & (j < sp), totals[j], 0.0)
                if j < m:
                    gap = gap + jnp.where(jnp.logical_not(wide) & (j > sp), totals[j], 0.0)
            used = (wide & (m < sp)) | (jnp.logical_not(wide) & (m > sp))
            state = state + jnp.where(used, jnp.exp(gap), 0.0) * st[m, h, 0:HEAD_DIM]
        queries = q_ref[rows].astype(F32)
        both = jnp.concatenate([queries * jnp.exp(cf), queries * jnp.exp(b_sum - eb)], axis=0)
        o = inner[h] + dot(state, both, NN, HIGH)
        o = o - jnp.mean(o, axis=0, keepdims=True)
        o = o * lax.rsqrt(jnp.mean(o * o, axis=0, keepdims=True) + 1e-06)
        gate = g_ref[rows].astype(F32)
        y = (o * (gate / (1.0 + jnp.exp(-gate)))).astype(BF16)
        yg[pl.ds(pl.multiple_of(tp * feats + h * HEAD_DIM, HEAD_DIM), HEAD_DIM)] = y
    y_args = (y_at, y_at(tp), y_s, y_r)
    gather_start(*y_args)

    for d in range(1, n_tp):
        source = lax.rem(tp + d, n_tp)
        remote(rt_ref, rts.at[source], rt_s.at[d - 1], rt_r.at[source], sp, source).wait_recv()
    info = rts[0]
    for j in range(1, n_tp):
        info = info + rts[j]
    experts = sel.shape[0]
    padded = (experts + 15) // 16 * 16
    expert = lax.broadcasted_iota(jnp.int32, (padded, length), 0).astype(F32)
    first, second = expert == info[0:1], expert == info[1:2]
    match = jnp.where(first | second, 1.0, 0.0)
    pair_weight = jnp.where(first, info[2:3], 0.0) + jnp.where(second, info[3:4], 0.0)
    rank = dot(match.astype(BF16), jnp.where(row < col, 1.0, 0.0).astype(BF16))
    place = lax.broadcasted_iota(jnp.int32, (slots, length), 0).astype(F32)
    slot_weight = []
    for e in range(experts):
        chosen = (place == rank[e:e + 1]) & (match[e:e + 1] > 0.0)
        sel[e] = jnp.where(chosen, 1.0, 0.0).astype(BF16)
        slot_weight.append(jnp.sum(jnp.where(chosen, pair_weight[e:e + 1], 0.0), axis=1, keepdims=True))

    gather_finish(*res_args)
    loads[0].wait()
    gather_forward(*y_args)
    gather_finish(*y_args)
    stream[...] = res[...].astype(F32) + dot(yg[...], wo[...], TN)
    s = stream[...]
    scale = lax.rsqrt(jnp.mean(s * s, axis=1, keepdims=True) + 1e-06)
    normed[...] = (s * scale * ng_ref[...].astype(F32)).astype(BF16)

    def x_copy(e, to, frm, send):
        return remote(xs.at[e, core], xr.at[frm, core], x_s.at[send], x_r.at[frm], to, tp)

    def dispatch(d, carry):
        e = lax.rem(sp + d, n_sp)
        for c in range(2):
            xs[e, c] = dot(sel[e], normed[:, c * half:(c + 1) * half]).astype(BF16)
        x_copy(e, e, sp, d - 1).start()
        return carry

    lax.fori_loop(1, n_sp, dispatch, 0)
    for c in range(2):
        xr[sp, c] = dot(sel[sp], normed[:, c * half:(c + 1) * half]).astype(BF16)
    for c in loads[1:]:
        c.wait()

    def f_copy(frm, part, send):
        return remote(xr.at[frm, part], xr.at[frm, part], f_s.at[send], f_r.at[frm], sp, partner)

    def p_copy(frm):
        return remote(pw.at[frm], pr.at[frm], p_s.at[frm], p_r.at[frm], sp, partner)

    def b_copy(frm, slot, send):
        return remote(rs.at[frm], rr.at[slot], b_s.at[send], b_r.at[slot], frm, tp)

    def expert_step(d, carry):
        frm = lax.rem(sp - d + n_sp, n_sp)

        @pl.when(d > 0)
        def _():
            x_copy(frm, frm, frm, d - 1).wait_recv()
            f_copy(frm, core, d - 1).start()
            f_copy(frm, 1 - core, d - 1).wait_recv()

        x0, x1 = xr[frm, 0], xr[frm, 1]
        gates = dot(x0, wg[0:half]) + dot(x1, wg[half:])
        ups = dot(x0, wu[0:half]) + dot(x1, wu[half:])
        hidden = (gates / (1.0 + jnp.exp(-gates)) * ups).astype(BF16)
        other = pl.multiple_of((1 - core) * half, half)
        mine = pl.multiple_of(core * half, half)
        pw[frm] = dot(hidden, wd[:, pl.ds(other, half)]).astype(BF16)
        p_copy(frm).start()
        kept = dot(hidden, wd[:, pl.ds(mine, half)])
        p_copy(frm).wait_recv()
        total = (kept + pr[frm].astype(F32)).astype(BF16)

        @pl.when(d > 0)
        def _():
            rs[frm] = total
            b_copy(frm, sp, d - 1).start()

        @pl.when(d == 0)
        def _():
            rr[sp] = total

        return carry

    lax.fori_loop(0, n_sp, expert_step, 0)

    for d in range(1, n_sp):
        source = lax.rem(sp + d, n_sp)
        b_copy(source, source, d - 1).wait_recv()
    for e in range(experts):
        weighted = (rr[e].astype(F32) * slot_weight[e]).astype(BF16)
        term = dot(sel[e], weighted, TN)
        if e == 0:
            zacc[...] = term
        else:
            zacc[...] += term
    zs[...] = zacc[...].astype(BF16)
    z_copies = []
    for d in range(1, n_tp):
        to = lax.rem(tp + d, n_tp)
        c = remote(zs.at[pl.ds(pl.multiple_of(to * tok, tok), tok)], zr.at[tp], z_s.at[d - 1], z_r.at[tp], sp, to)
        c.start()
        z_copies.append(c)
    own = pl.ds(pl.multiple_of(tp * tok, tok), tok)
    zr[tp] = zs[own]
    for d in range(1, n_tp):
        source = lax.rem(tp + d, n_tp)
        remote(zs.at[own], zr.at[source], z_s.at[d - 1], z_r.at[source], sp, source).wait_recv()
    for c in range(2):
        total = stream[own, c * half:(c + 1) * half]
        for i in range(chips):
            total = total + zr[2 * i + c].astype(F32)
        out_ref[:, c * half:(c + 1) * half] = total.astype(BF16)

    for c in rt_copies + st_copies + z_copies:
        c.wait_send()
    gather_drain(*res_args)
    gather_drain(*y_args)

    def drain(d, carry):
        frm = lax.rem(sp - d + n_sp, n_sp)
        p_copy(frm).wait_send()

        @pl.when(d > 0)
        def _():
            x_copy(frm, frm, frm, d - 1).wait_send()
            f_copy(frm, core, d - 1).wait_send()
            b_copy(frm, sp, d - 1).wait_send()

        return carry

    lax.fori_loop(0, n_sp, drain, 0)


def on_device(
    query_input, key_input, retrieved_content_matrix, gate_input, log_decay, residual, out_weight,
    norm_gain, routes, route_weight, gate_weight, up_weight, down_weight,
):
    n_sp, n_tp = lax.axis_size("sp"), lax.axis_size("tp")
    feats, length = query_input.shape
    heads = feats // HEAD_DIM
    tok, picks = routes.shape
    width = residual.shape[1]
    half = width // 2
    experts = n_sp * gate_weight.shape[0]
    ff = gate_weight.shape[2]
    capacity = (5 * tok + 2 * experts - 1) // (2 * experts)
    slots = (capacity * n_tp + 15) // 16 * 16
    ld = jnp.pad(log_decay.reshape(2 * heads, length), ((0, 8 - 2 * heads), (0, 0)))
    info = jnp.concatenate([routes.astype(F32).T, route_weight.T, jnp.zeros((4, tok), F32)], axis=0)
    mine = (jnp.arange(n_tp) == lax.axis_index("tp"))[None, :, None]
    rt = jnp.where(mine, info[:, None, :], 0.0).reshape(8, n_tp * tok)
    vm, dma = pltpu.VMEM, pltpu.SemaphoreType.DMA
    ns, nt = (n_sp,), (n_tp,)
    return pl.pallas_call(
        functools.partial(kernel, n_sp, n_tp, slots),
        out_shape=jax.ShapeDtypeStruct((tok, width), BF16),
        in_specs=[pl.BlockSpec(memory_space=vm)] * 8 + [pl.BlockSpec(memory_space=pl.ANY)] * 4,
        out_specs=pl.BlockSpec(memory_space=vm),
        scratch_shapes=[
            vm(out_weight.shape, BF16), vm((width, ff), BF16), vm((width, ff), BF16), vm((ff, width), BF16),
            vm((n_sp, heads, HEAD_DIM + 8, 2 * HEAD_DIM), F32),
            vm((n_tp * feats, length), BF16),
            vm((n_tp * tok, width), BF16),
            vm((n_tp, 8, length), F32),
            vm((length, width), F32), vm((length, width), BF16),
            vm((experts, slots, length), BF16),
            vm((n_sp, 2, slots, half), BF16), vm((n_sp, 2, slots, half), BF16),
            vm((n_sp, slots, half), BF16), vm((n_sp, slots, half), BF16),
            vm((n_sp, slots, half), BF16), vm((n_sp, slots, half), BF16),
            vm((length, half), F32), vm((length, half), BF16), vm((n_tp, tok, half), BF16),
            dma((4,)), dma(ns), dma(ns), dma(nt), dma(nt), dma(nt), dma(nt), dma(nt), dma(nt),
            dma(ns), dma(ns), dma(ns), dma(ns), dma(ns), dma(ns), dma(ns), dma(ns), dma(nt), dma(nt),
        ],
        compiler_params=pltpu.CompilerParams(
            collective_id=0, has_side_effects=True, vmem_limit_bytes=60 * 1024 * 1024
        ),
    )(
        query_input, key_input, retrieved_content_matrix, gate_input, ld, rt, residual,
        norm_gain.reshape(1, -1), out_weight, gate_weight, up_weight, down_weight,
    )


def solution(mesh):
    placed = (
        P("tp", "sp"), P("tp", "sp"), P("tp", "sp"), P("tp", "sp"), P(None, "tp", "sp"),
        P(("sp", "tp"), None), P(), P(), P(("sp", "tp"), None), P(("sp", "tp"), None),
        P("sp", None, "tp"), P("sp", None, "tp"), P("sp", "tp", None),
    )
    return jax.shard_map(
        on_device, mesh=mesh, in_specs=placed, out_specs=P(("sp", "tp"), None), check_vma=False
    )
```

time: 206 us -> 101 us (0.49); the launches traced: 202 us -> 100 us
  Pallas kernels: 0 us -> 86.3 us
  waiting for transfers between devices: 84.5 us -> 0 us
  blocking collectives: 31.7 us -> 0 us
  matrix products: 26.6 us -> 0 us
  starting transfers between devices: 15.5 us -> 0 us
  between operations: 14.3 us -> 0.02 us
  local copies, waits for them, and re-layouts: 20.4 us -> 11.9 us
  other arithmetic: 9.16 us -> 2.18 us
    pallas_call x0 -> x1, Pallas kernels: none -> 86.3 us  [on_device(): pl.pallas_call(functools.partial(kernel, n_sp, n_tp, slots), out_shape=ja...]
    reduce_scatter x1 -> x0, waiting for transfers between devices: 39.2 us -> none  [on_device(): lax.psum_scatter(terms.astype(jnp.bfloat16), 'tp', scatter_dimension=0, t...]
    all_gather x1 -> x0, waiting for transfers between devices: 37.5 us -> none  [on_device(): piece = lax.all_gather(received, 'tp', axis=0, tiled=True)]
    dot_general x9 -> x0, matrix products: 26.6 us -> none  [the longest x1 13 us: on_device(): jnp.dot(hidden, down_weight[0], preferred_element_type=jnp.float32)]
    all_to_all x2 -> x0, starting transfers between devices: 15.2 us -> none  [the longest x1 11.1 us: on_device(): lax.all_to_all(mixer_out, 'tp', split_axis=1, concat_axis=0, tiled=True)]
    all_gather x2 -> x0, blocking collectives: 13.2 us -> none  [entering(): pieces = jax.tree.map(lambda part: lax.all_gather(part, axis), value)]
    all_to_all x1 -> x0, blocking collectives: 10 us -> none  [on_device(): lax.all_to_all(send_rows, 'sp', split_axis=0, concat_axis=0, tiled=True)]
    unnamed x1 -> x0, blocking collectives: 8.44 us -> none
  transfers between devices with their start and end apart: 4 -> 0, of which waited for: 4 -> 0; matrix products, arithmetic and copies ran while one was open for 1% -> 0% of each run, Pallas kernels for 0% -> 0%
where the time goes in v1:
time: 101 us; the launch traced here: 100 us
  Pallas kernels  86.3 us (85%)
  local copies, waits for them, and re-layouts  11.9 us (12%)
  other arithmetic  2.18 us (2%)
    pallas_call x1, Pallas kernels, on_device(): pl.pallas_call(functools.partial(kernel, n_sp, n_tp, slots), out_shape=ja...  86.3 us
    unnamed x5, local copies, waits for them, and re-layouts  8.99 us

profile of v1, /device:TPU:25, one launch (start us, length us, event | category | flops | bytes accessed | tf_op | source)
XLA Modules:
  0.0 100.4 jit_solution(3197682728315584746)
XLA Ops:
  0.0 0.0 copy-start
  0.0 0.1 broadcast_in_dim.31
  0.1 0.1 broadcast_in_dim.32
  0.2 0.1 pad.7.clone
  0.3 0.8 convert_bitcast_fusion
  1.1 0.7 maximum_maximum_fusion
  1.8 0.7 reshape.14
  2.5 0.6 pad.4.ld_ref
  3.1 1.3 %reshape.15.ng_ref = bf16[1,2048]{1,0:T(2,128)(2,1)} reshape(bf16[2048]{0:T(1024)(128)(2,1)} %param.20) | data formatting | bytes 8192 | tf_op jit(solution)/shard_map/reshape | solution.py:341
  4.4 0.1 broadcast_in_dim.36
  4.5 0.6 broadcast_select_fusion.rt_ref
  5.1 4.6 %copy.14.wg_hbm = bf16[1,2048,688]{2,1,0:T(8,128)(2,1)} copy(bf16[1,2048,688]{1,2,0:T(8,128)(2,1)} %param.23) | data formatting | bytes 5636096 | tf_op args[10]
  9.7 0.0 copy-done
  9.7 2.8 %copy.15.wu_hbm = bf16[1,2048,688]{2,1,0:T(8,128)(2,1)} copy(bf16[1,2048,688]{1,2,0:T(8,128)(2,1)S(1)} %copy-done) | data formatting | bytes 5636096 | tf_op args[11]
  12.5 86.3 %shard_map.127 = bf16[32,2048]{1,0:T(8,128)(2,1)} custom-call(bf16[128,256]{1,0:T(8,128)(2,1)} %q_ref.1, bf16[128,256]{1,0:T(8,128)(2,1)} %k_ref.1, bf16[128,256]{1,0:T(8,128)(2,1)} %v_ref.1, bf16[128,256]{1,0:T(8,128)(2,1)} %g_ref.1, f32[8,256]{1,0:T(8,128)} %pad.4.ld_ref, f32[8,256]{1,0:T(8,128)} %broadcast_select_fusion.rt_ref, bf16[32,2048]{1,0:T(8,128)(2,1)} %res_ref.1, ...), custom_call_target="tpu_custom_call" | custom-call | tf_op jit(solution)/shard_map/pallas_call | solution.py:316
  98.8 1.6 %copy.17 = bf16[32,2048]{1,0:T(8,128)(2,1)} copy(bf16[32,2048]{1,0:T(8,128)(2,1)} %shard_map.127) | data formatting | bytes 262144
  (3 shorter events, 0.0 us)
Async XLA Ops:
  0.0 9.7 %copy-start = (bf16[1,2048,688]{1,2,0:T(8,128)(2,1)S(1)}, bf16[1,2048,688]{1,2,0:T(8,128)(2,1)}, u32[]{:S(2)}) copy-start(bf16[1,2048,688]{1,2,0:T(8,128)(2,1)} %param.24) | copy-start | bytes 8454148

commit v2 on v1

--- a/solution.py
+++ b/solution.py
@@ -22,9 +22,9 @@
 
 def kernel(
     n_sp, n_tp, slots,
-    q_ref, k_ref, v_ref, g_ref, ld_ref, rt_ref, res_ref, ng_ref, wo_hbm, wg_hbm, wu_hbm, wd_hbm,
+    q_ref, k_ref, v_ref, g_ref, ld_ref, routes_ref, weights_ref, res_ref, ng_ref, wo_hbm, wg_hbm, wu_hbm, wd_hbm,
     out_ref,
-    wo, wg, wu, wd, st, yg, res, rts, stream, normed, sel, xs, xr, pw, pr, rs, rr, zacc, zs, zr,
+    wo, wg, wu, wd, ld_all, rt_ref, st, yg, res, rts, stream, normed, sel, xs, xr, hid, kept, pw, pr, rs, rr, zacc, zs, zr,
     wsem, st_s, st_r, y_s, y_r, res_s, res_r, rt_s, rt_r, x_s, x_r, f_s, f_r, p_s, p_r, b_s, b_r, z_s, z_r,
 ):
     sp, tp = lax.axis_index("sp"), lax.axis_index("tp")
@@ -35,6 +35,7 @@
     heads = feats // HEAD_DIM
     tok = res_ref.shape[0]
     half = wo.shape[1] // 2
+    quarter = half // 2
 
     def remote(src, dst, send, recv, to_sp, to_tp):
         return pltpu.make_async_remote_copy(
@@ -82,6 +83,14 @@
     def y_at(i):
         return yg.at[pl.ds(pl.multiple_of(i * feats, feats), feats)]
 
+    ld_all[...] = jnp.zeros_like(ld_all)
+    ld_all[0:heads] = ld_ref[0]
+    ld_all[heads:2 * heads] = ld_ref[1]
+    token = lax.broadcasted_iota(jnp.int32, (tok, length), 0) + tp * tok
+    spread = jnp.where(token == lax.broadcasted_iota(jnp.int32, (tok, length), 1), 1.0, 0.0)
+    rt_ref[...] = jnp.zeros_like(rt_ref)
+    rt_ref[0:2] = dot(routes_ref[...].astype(F32), spread, NN, HIGH)
+    rt_ref[2:4] = dot(weights_ref[...], spread, NN, HIGH)
     pl.semaphore_wait(barrier, n_tp - 1 + n_sp - 1)
     res_args = (res_at, res_ref, res_s, res_r)
     gather_start(*res_args)
@@ -96,7 +105,7 @@
 
     row = lax.broadcasted_iota(jnp.int32, (length, length), 0)
     col = lax.broadcasted_iota(jnp.int32, (length, length), 1)
-    ld = ld_ref[...]
+    ld = ld_all[...]
     upto = dot(ld, (row <= col).astype(F32), precision=HIGH)
     before = upto - ld
     upto_t, before_t = upto.T, before.T
@@ -126,7 +135,6 @@
         weight = weight + jnp.exp(jnp.where(row <= col, eb - eb_t, -jnp.inf))
         inner.append(dot(v_ref[rows], (scores * weight).astype(BF16), NT))
 
-    gather_forward(*res_args)
     for d in range(1, n_sp):
         source = lax.rem(sp + d, n_sp)
         remote(st.at[source], st.at[source], st_s.at[d - 1], st_r.at[source], source, tp).wait_recv()
@@ -156,6 +164,7 @@
         yg[pl.ds(pl.multiple_of(tp * feats + h * HEAD_DIM, HEAD_DIM), HEAD_DIM)] = y
     y_args = (y_at, y_at(tp), y_s, y_r)
     gather_start(*y_args)
+    gather_forward(*res_args)
 
     for d in range(1, n_tp):
         source = lax.rem(tp + d, n_tp)
@@ -177,22 +186,21 @@
         sel[e] = jnp.where(chosen, 1.0, 0.0).astype(BF16)
         slot_weight.append(jnp.sum(jnp.where(chosen, pair_weight[e:e + 1], 0.0), axis=1, keepdims=True))
 
-    gather_finish(*res_args)
     loads[0].wait()
     gather_forward(*y_args)
+    gather_finish(*res_args)
     gather_finish(*y_args)
     stream[...] = res[...].astype(F32) + dot(yg[...], wo[...], TN)
     s = stream[...]
     scale = lax.rsqrt(jnp.mean(s * s, axis=1, keepdims=True) + 1e-06)
-    normed[...] = (s * scale * ng_ref[...].astype(F32)).astype(BF16)
+    normed[...] = (s * scale * ng_ref[...].astype(F32)[None, :]).astype(BF16)
 
     def x_copy(e, to, frm, send):
-        return remote(xs.at[e, core], xr.at[frm, core], x_s.at[send], x_r.at[frm], to, tp)
+        return remote(xs.at[e], xr.at[frm, core], x_s.at[send], x_r.at[frm], to, tp)
 
     def dispatch(d, carry):
         e = lax.rem(sp + d, n_sp)
-        for c in range(2):
-            xs[e, c] = dot(sel[e], normed[:, c * half:(c + 1) * half]).astype(BF16)
+        xs[e] = dot(sel[e], normed[:, pl.ds(pl.multiple_of(core * half, half), half)]).astype(BF16)
         x_copy(e, e, sp, d - 1).start()
         return carry
 
@@ -205,11 +213,36 @@
     def f_copy(frm, part, send):
         return remote(xr.at[frm, part], xr.at[frm, part], f_s.at[send], f_r.at[frm], sp, partner)
 
-    def p_copy(frm):
-        return remote(pw.at[frm], pr.at[frm], p_s.at[frm], p_r.at[frm], sp, partner)
-
-    def b_copy(frm, slot, send):
-        return remote(rs.at[frm], rr.at[slot], b_s.at[send], b_r.at[slot], frm, tp)
+    def p_copy(i):
+        return remote(pw.at[i], pr.at[i], p_s.at[i], p_r.at[i], sp, partner)
+
+    def b_copy(part, to, slot, send):
+        i = part * n_sp
+        return remote(rs.at[i + to], rr.at[i + slot], b_s.at[i + send], b_r.at[i + slot], to, tp)
+
+    def give_back(d, part, hidden):
+        frm = lax.rem(sp - d + n_sp, n_sp)
+        i = part * n_sp + frm
+        other = pl.multiple_of((1 - core) * half + part * quarter, quarter)
+        mine = pl.multiple_of(core * half + part * quarter, quarter)
+        pw[i] = dot(hidden, wd[:, pl.ds(other, quarter)]).astype(BF16)
+        p_copy(i).start()
+        kept[i] = dot(hidden, wd[:, pl.ds(mine, quarter)])
+
+    def finish(d, part):
+        frm = lax.rem(sp - d + n_sp, n_sp)
+        i = part * n_sp + frm
+        p_copy(i).wait_recv()
+        total = (kept[i] + pr[i].astype(F32)).astype(BF16)
+
+        @pl.when(d > 0)
+        def _():
+            rs[i] = total
+            b_copy(part, frm, sp, d - 1).start()
+
+        @pl.when(d == 0)
+        def _():
+            rr[i] = total
 
     def expert_step(d, carry):
         frm = lax.rem(sp - d + n_sp, n_sp)
@@ -221,57 +254,69 @@
             f_copy(frm, 1 - core, d - 1).wait_recv()
 
         x0, x1 = xr[frm, 0], xr[frm, 1]
-        gates = dot(x0, wg[0:half]) + dot(x1, wg[half:])
-        ups = dot(x0, wu[0:half]) + dot(x1, wu[half:])
+        gates = dot(x0, wg[:, 0:half], NT) + dot(x1, wg[:, half:], NT)
+        ups = dot(x0, wu[:, 0:half], NT) + dot(x1, wu[:, half:], NT)
         hidden = (gates / (1.0 + jnp.exp(-gates)) * ups).astype(BF16)
-        other = pl.multiple_of((1 - core) * half, half)
-        mine = pl.multiple_of(core * half, half)
-        pw[frm] = dot(hidden, wd[:, pl.ds(other, half)]).astype(BF16)
-        p_copy(frm).start()
-        kept = dot(hidden, wd[:, pl.ds(mine, half)])
-        p_copy(frm).wait_recv()
-        total = (kept + pr[frm].astype(F32)).astype(BF16)
+        hid[frm] = hidden
+        give_back(d, 0, hidden)
 
         @pl.when(d > 0)
         def _():
-            rs[frm] = total
-            b_copy(frm, sp, d - 1).start()
+            finish(d - 1, 0)
+
+        return carry
+
+    def second_step(d, carry):
+        give_back(d, 1, hid[lax.rem(sp - d + n_sp, n_sp)])
 
         @pl.when(d == 0)
         def _():
-            rr[sp] = total
+            finish(n_sp - 1, 0)
+
+        @pl.when(d > 0)
+        def _():
+            finish(d - 1, 1)
 
         return carry
 
     lax.fori_loop(0, n_sp, expert_step, 0)
-
-    for d in range(1, n_sp):
-        source = lax.rem(sp + d, n_sp)
-        b_copy(source, source, d - 1).wait_recv()
-    for e in range(experts):
-        weighted = (rr[e].astype(F32) * slot_weight[e]).astype(BF16)
-        term = dot(sel[e], weighted, TN)
-        if e == 0:
-            zacc[...] = term
-        else:
-            zacc[...] += term
-    zs[...] = zacc[...].astype(BF16)
+    lax.fori_loop(0, n_sp, second_step, 0)
+    finish(n_sp - 1, 1)
+
+    own = pl.ds(pl.multiple_of(tp * tok, tok), tok)
     z_copies = []
-    for d in range(1, n_tp):
-        to = lax.rem(tp + d, n_tp)
-        c = remote(zs.at[pl.ds(pl.multiple_of(to * tok, tok), tok)], zr.at[tp], z_s.at[d - 1], z_r.at[tp], sp, to)
-        c.start()
-        z_copies.append(c)
-    own = pl.ds(pl.multiple_of(tp * tok, tok), tok)
-    zr[tp] = zs[own]
-    for d in range(1, n_tp):
-        source = lax.rem(tp + d, n_tp)
-        remote(zs.at[own], zr.at[source], z_s.at[d - 1], z_r.at[source], sp, source).wait_recv()
-    for c in range(2):
-        total = stream[own, c * half:(c + 1) * half]
-        for i in range(chips):
-            total = total + zr[2 * i + c].astype(F32)
-        out_ref[:, c * half:(c + 1) * half] = total.astype(BF16)
+    for part in range(2):
+        for d in range(1, n_sp):
+            source = lax.rem(sp + d, n_sp)
+            b_copy(part, source, source, d - 1).wait_recv()
+        for e in range(experts):
+            weighted = (rr[part * n_sp + e].astype(F32) * slot_weight[e]).astype(BF16)
+            term = dot(sel[e], weighted, TN)
+            if e == 0:
+                zacc[...] = term
+            else:
+                zacc[...] += term
+        zs[part] = zacc[...].astype(BF16)
+        for d in range(1, n_tp):
+            to = lax.rem(tp + d, n_tp)
+            c = remote(
+                zs.at[part, pl.ds(pl.multiple_of(to * tok, tok), tok)], zr.at[part * n_tp + tp],
+                z_s.at[part * n_tp + d - 1], z_r.at[part * n_tp + tp], sp, to,
+            )
+            c.start()
+            z_copies.append(c)
+        zr[part * n_tp + tp] = zs[part, own]
+    for part in range(2):
+        for d in range(1, n_tp):
+            source = lax.rem(tp + d, n_tp)
+            i = part * n_tp + source
+            remote(zs.at[part, own], zr.at[i], z_s.at[part * n_tp + d - 1], z_r.at[i], sp, source).wait_recv()
+        for c in range(2):
+            columns = slice(c * half + part * quarter, c * half + (part + 1) * quarter)
+            total = stream[own, columns]
+            for i in range(chips):
+                total = total + zr[part * n_tp + 2 * i + c].astype(F32)
+            out_ref[:, columns] = total.astype(BF16)
 
     for c in rt_copies + st_copies + z_copies:
         c.wait_send()
@@ -281,12 +326,14 @@
     def drain(d, carry):
         frm = lax.rem(sp - d + n_sp, n_sp)
         p_copy(frm).wait_send()
+        p_copy(n_sp + frm).wait_send()
 
         @pl.when(d > 0)
         def _():
             x_copy(frm, frm, frm, d - 1).wait_send()
             f_copy(frm, core, d - 1).wait_send()
-            b_copy(frm, sp, d - 1).wait_send()
+            b_copy(0, frm, sp, d - 1).wait_send()
+            b_copy(1, frm, sp, d - 1).wait_send()
 
         return carry
 
@@ -307,38 +354,39 @@
     ff = gate_weight.shape[2]
     capacity = (5 * tok + 2 * experts - 1) // (2 * experts)
     slots = (capacity * n_tp + 15) // 16 * 16
-    ld = jnp.pad(log_decay.reshape(2 * heads, length), ((0, 8 - 2 * heads), (0, 0)))
-    info = jnp.concatenate([routes.astype(F32).T, route_weight.T, jnp.zeros((4, tok), F32)], axis=0)
-    mine = (jnp.arange(n_tp) == lax.axis_index("tp"))[None, :, None]
-    rt = jnp.where(mine, info[:, None, :], 0.0).reshape(8, n_tp * tok)
     vm, dma = pltpu.VMEM, pltpu.SemaphoreType.DMA
     ns, nt = (n_sp,), (n_tp,)
     return pl.pallas_call(
         functools.partial(kernel, n_sp, n_tp, slots),
         out_shape=jax.ShapeDtypeStruct((tok, width), BF16),
-        in_specs=[pl.BlockSpec(memory_space=vm)] * 8 + [pl.BlockSpec(memory_space=pl.ANY)] * 4,
+        in_specs=[pl.BlockSpec(memory_space=vm)] * 9 + [pl.BlockSpec(memory_space=pl.ANY)] * 4,
         out_specs=pl.BlockSpec(memory_space=vm),
         scratch_shapes=[
-            vm(out_weight.shape, BF16), vm((width, ff), BF16), vm((width, ff), BF16), vm((ff, width), BF16),
+            vm(out_weight.shape, BF16), vm((ff, width), BF16), vm((ff, width), BF16), vm((ff, width), BF16),
+            vm((8, length), F32), vm((8, length), F32),
             vm((n_sp, heads, HEAD_DIM + 8, 2 * HEAD_DIM), F32),
             vm((n_tp * feats, length), BF16),
             vm((n_tp * tok, width), BF16),
             vm((n_tp, 8, length), F32),
             vm((length, width), F32), vm((length, width), BF16),
             vm((experts, slots, length), BF16),
-            vm((n_sp, 2, slots, half), BF16), vm((n_sp, 2, slots, half), BF16),
-            vm((n_sp, slots, half), BF16), vm((n_sp, slots, half), BF16),
-            vm((n_sp, slots, half), BF16), vm((n_sp, slots, half), BF16),
-            vm((length, half), F32), vm((length, half), BF16), vm((n_tp, tok, half), BF16),
+            vm((n_sp, slots, half), BF16), vm((n_sp, 2, slots, half), BF16),
+            vm((n_sp, slots, ff), BF16), vm((2 * n_sp, slots, half // 2), F32),
+            vm((2 * n_sp, slots, half // 2), BF16), vm((2 * n_sp, slots, half // 2), BF16),
+            vm((2 * n_sp, slots, half // 2), BF16), vm((2 * n_sp, slots, half // 2), BF16),
+            vm((length, half // 2), F32), vm((2, length, half // 2), BF16), vm((2 * n_tp, tok, half // 2), BF16),
             dma((4,)), dma(ns), dma(ns), dma(nt), dma(nt), dma(nt), dma(nt), dma(nt), dma(nt),
-            dma(ns), dma(ns), dma(ns), dma(ns), dma(ns), dma(ns), dma(ns), dma(ns), dma(nt), dma(nt),
+            dma(ns), dma(ns), dma(ns), dma(ns), dma((2 * n_sp,)), dma((2 * n_sp,)),
+            dma((2 * n_sp,)), dma((2 * n_sp,)), dma((2 * n_tp,)), dma((2 * n_tp,)),
         ],
         compiler_params=pltpu.CompilerParams(
             collective_id=0, has_side_effects=True, vmem_limit_bytes=60 * 1024 * 1024
         ),
     )(
-        query_input, key_input, retrieved_content_matrix, gate_input, ld, rt, residual,
-        norm_gain.reshape(1, -1), out_weight, gate_weight, up_weight, down_weight,
+        query_input, key_input, retrieved_content_matrix, gate_input, log_decay, routes.T, route_weight.T,
+        residual,
+        norm_gain, out_weight, jnp.swapaxes(gate_weight, 1, 2), jnp.swapaxes(up_weight, 1, 2),
+        down_weight,
     )
 
 

time: 101 us -> 77.9 us (0.77)
  Pallas kernels: 86.3 us -> 75.7 us
  local copies, waits for them, and re-layouts: 11.9 us -> 1.57 us
  other arithmetic: 2.18 us -> 0 us
    pallas_call x1, Pallas kernels: 86.3 us -> 75.7 us  [on_device(): pl.pallas_call(functools.partial(kernel, n_sp, n_tp, slots), out_shape=ja...]
    unnamed x5 -> x1, local copies, waits for them, and re-layouts: 8.99 us -> 1.57 us
    reshape x2 -> x0, local copies, waits for them, and re-layouts: 1.99 us -> none  [the longest x1 1.29 us: on_device(): norm_gain.reshape(1, -1)]
where the time goes in v2:
time: 77.9 us; the launch traced here: 77.2 us
  Pallas kernels  75.7 us (97%)
  local copies, waits for them, and re-layouts  1.57 us (2%)
    pallas_call x1, Pallas kernels, on_device(): pl.pallas_call(functools.partial(kernel, n_sp, n_tp, slots), out_shape=ja...  75.7 us
    unnamed x1, local copies, waits for them, and re-layouts  1.57 us

profile of v2, /device:TPU:25, one launch (start us, length us, event | category | flops | bytes accessed | tf_op | source)
XLA Modules:
  0.0 77.2 jit_solution(14044426271478741517)
XLA Ops:
  0.0 75.7 %shard_map.127 = bf16[32,2048]{1,0:T(8,128)(2,1)} custom-call(bf16[128,256]{1,0:T(8,128)(2,1)} %q_ref.1, bf16[128,256]{1,0:T(8,128)(2,1)} %k_ref.1, bf16[128,256]{1,0:T(8,128)(2,1)} %v_ref.1, bf16[128,256]{1,0:T(8,128)(2,1)} %g_ref.1, f32[2,2,256]{2,1,0:T(2,128)} %ld_ref.1, s32[2,32]{1,0:T(2,128)} %bitcast.6, f32[2,32]{1,0:T(2,128)} %bitcast.7, ...), custom_call_target="tpu_custom_call" | custom-call | tf_op jit(solution)/shard_map/pallas_call | solution.py:359
  75.7 1.6 %copy.15 = bf16[32,2048]{1,0:T(8,128)(2,1)} copy(bf16[32,2048]{1,0:T(8,128)(2,1)} %shard_map.127) | data formatting | bytes 262144
